TPU v7x, 512 devices: a whole 4x4x16 slice. The times are simulated.
512 devices in a mesh: fs: 16 (over y, x), tp: 32 (over z, core).
Axes of the slice: x: 4, y: 4, z: 16, core: 2. Of those that a mesh axis runs over, the one named last changes fastest.
Arguments:
- normed: bfloat16 [2048, 49152], P('tp', 'fs'), may hold values from -6 to 6
- key_cot: bfloat16 [2048, 49152], P('tp', 'fs'), may hold values from -6 to 6
- first_map: bfloat16 [2048, 49152], P('tp', 'fs'), may hold values from -6 to 6
- second_map: bfloat16 [2048, 49152], P('tp', 'fs'), may hold values from -6 to 6
- lambdas: float32 [8], replicated, may hold values from 0.3 to 0.8
- factor: bfloat16 [2048, 256], replicated, may hold values from -0.125 to 0.125
- key_master: float32 [2048, 2048], P('fs', 'tp'), may hold values from -0.125 to 0.125
- value_master: float32 [2048, 2048], P('fs', 'tp'), may hold values from -0.125 to 0.125
- key_first: float32 [256, 2048], P('fs', 'tp'), may hold values from -6 to 6
- key_second: float32 [256, 2048], P('fs', 'tp'), may hold values from 0.5 to 2
- value_first: float32 [256, 2048], P('fs', 'tp'), may hold values from -6 to 6
- value_second: float32 [256, 2048], P('fs', 'tp'), may hold values from 0.5 to 2
Outputs:
- key_master_new: float32 [2048, 2048], P('fs', 'tp')
- value_master_new: float32 [2048, 2048], P('fs', 'tp')
- key_copy: bfloat16 [2048, 2048], P(None, 'tp')
- value_copy: bfloat16 [2048, 2048], P(None, 'tp')
- key_first_new: float32 [256, 2048], P('fs', 'tp')
- key_second_new: float32 [256, 2048], P('fs', 'tp')
- value_first_new: float32 [256, 2048], P('fs', 'tp')
- value_second_new: float32 [256, 2048], P('fs', 'tp')
All inputs are finite; a program needn't handle non-finite values.
Results may differ from a plain program's by a relative error of at most 0.0012.
Values may be sent and summed in bfloat16 or wider, within the bound.
No kernel may reach another device: no remote copies, remote signals or barrier semaphores. Data moves between devices by JAX's collectives and lax.ppermute only.
A program may use at most 64 MiB of HBM per device.

v0:
```python
import math
import jax
import jax.numpy as jnp
from jax import lax
from jax.sharding import Mesh
from jax.sharding import PartitionSpec as P

VALUE_DIM = 256
TP = ("tp_0", "tp_1")
FS = ("fs_0", "fs_1")
FS_TP = ("fs_0", "fs_1", "tp_0", "tp_1")


def cut_along(shard, dim, size):
    lengths = shard.shape
    pieces = shard.reshape(*lengths[:dim], size, lengths[dim] // size, *lengths[dim + 1 :])
    return jnp.moveaxis(pieces, dim, 0)


def summed_on_arrival(shard, axis, dim):
    size = lax.axis_size(axis)
    pieces = lax.all_to_all(cut_along(shard, dim, size), axis, 0, 0, tiled=True)
    return jnp.sum(pieces, axis=0)


def sent_to_all(shard, axis):
    size = lax.axis_size(axis)
    return lax.all_to_all(
        jnp.broadcast_to(shard[None], (size, *shard.shape)), axis, 0, 0, tiled=True
    )


def in_order(pieces, dim):
    lengths = list(pieces.shape[1:])
    lengths[dim] *= pieces.shape[0]
    return jnp.moveaxis(pieces, 0, dim).reshape(lengths)


def collect(shard, axis, dim):
    pieces = sent_to_all(shard, axis)
    return in_order(pieces, dim)


def over_axes(shard, axes):
    for axis in axes:
        shard = lax.psum(shard, axis)
    return shard


def local(
    normed,
    key_cot,
    first_map,
    second_map,
    lambdas,
    factor,
    key_master,
    value_master,
    key_first,
    key_second,
    value_first,
    value_second,
):
    width = first_map.shape[0]
    key_width = key_cot.shape[0]
    heads = lambdas.shape[0]
    tok_local = normed.shape[1]
    rows_here = lax.axis_index(TP) * width + lax.iota(jnp.int32, width)
    owners = rows_here // VALUE_DIM
    picked = (owners[:, None] == lax.iota(jnp.int32, heads)[None, :]).astype(jnp.float32)
    row_lambda = jnp.sum(picked * lambdas[None, :], axis=1)
    value_cot = (
        first_map.astype(jnp.float32) - row_lambda[:, None] * second_map.astype(jnp.float32)
    ).astype(jnp.bfloat16)
    cotangents = jnp.concatenate([key_cot, value_cot], axis=0)
    norm_scale = 1.0 / math.sqrt(tok_local * lax.axis_size(FS))
    fs_rows = key_master.shape[0]
    factor_rows = lax.dynamic_slice_in_dim(factor, lax.axis_index(FS) * fs_rows, fs_rows, 0).astype(
        jnp.float32
    )
    term = lax.dot_general(
        lax.all_gather(normed, TP, axis=0, tiled=True),
        cotangents,
        (((1,), (1,)), ((), ())),
        preferred_element_type=jnp.float32,
    )
    gradient = summed_on_arrival(term, FS, 0) * norm_scale
    partial_value = lax.dot_general(
        factor_rows, gradient, (((0,), (0,)), ((), ())), precision=lax.Precision.HIGHEST
    )
    small = summed_on_arrival(partial_value, FS, 0)
    first = jnp.concatenate([key_first, value_first], axis=1)
    second = jnp.concatenate([key_second, value_second], axis=1)
    first_new = 0.8 * first + 0.2 * small
    second_new = 0.9 * second + 0.1 * small * small
    direction = first_new / (jnp.sqrt(second_new) + 1e-06)
    directions = collect(direction, FS, 0)
    raw = jnp.dot(factor_rows, directions, precision=lax.Precision.HIGHEST)
    key_raw = raw[:, :key_width]
    value_raw = raw[:, key_width:]
    squares = (
        over_axes(jnp.sum(key_raw * key_raw), FS_TP),
        over_axes(jnp.sum(value_raw * value_raw), FS_TP),
    )
    key_cells = fs_rows * lax.axis_size(FS) * key_width * lax.axis_size(TP)
    value_cells = fs_rows * lax.axis_size(FS) * width * lax.axis_size(TP)
    key_update = key_raw / jnp.sqrt(squares[0] / key_cells + 0.01)
    value_update = value_raw / jnp.sqrt(squares[1] / value_cells + 0.01)
    key_new = 0.998 * key_master - 0.02 * key_update
    value_new = 0.998 * value_master - 0.02 * value_update
    halves = jnp.concatenate([key_new, value_new], axis=1).astype(jnp.bfloat16)
    copies = collect(halves, FS, 0)
    return (
        key_new,
        value_new,
        copies[:, :key_width],
        copies[:, key_width:],
        first_new[:, :key_width],
        second_new[:, :key_width],
        first_new[:, key_width:],
        second_new[:, key_width:],
    )


def solution(mesh):
    split = Mesh(mesh.devices.reshape(4, 4, 16, 2), ("fs_0", "fs_1", "tp_0", "tp_1"))
    placed = (
        P(TP, FS),
        P(TP, FS),
        P(TP, FS),
        P(TP, FS),
        P(),
        P(),
        P(FS, TP),
        P(FS, TP),
        P(FS, TP),
        P(FS, TP),
        P(FS, TP),
        P(FS, TP),
    )
    return jax.shard_map(
        local,
        mesh=split,
        in_specs=placed,
        out_specs=(
            P(FS, TP),
            P(FS, TP),
            P(None, TP),
            P(None, TP),
            P(FS, TP),
            P(FS, TP),
            P(FS, TP),
            P(FS, TP),
        ),
        check_vma=False,
    )
```

profile of v0, /device:TPU:1, one launch (start us, length us, event | category | flops | bytes accessed | tf_op | source)
XLA Modules:
  0.0 239.1 jit_solution(16993545285375096101)
XLA Ops:
  7.3 0.7 all-gather.2.cloned.1.call-update
  8.0 0.7 select_reduce_fusion
  8.7 1.3 subtract_convert_fusion
  10.0 92.9 %all-gather.2.cloned.1.call-done = bf16[2048,3072]{1,0:T(8,128)(2,1)} async-done(((bf16[64,3072]{1,0:T(8,128)(2,1)}), bf16[2048,3072]{1,0:T(8,128)(2,1)}) %all-gather.2.cloned.1.call-update) | async-done | bytes 12582928 | tf_op jit(solution)/shard_map/all_gather | solution.py:82
  103.0 9.0 %convolution_bitcast_fusion = f32[16,16,8,128]{3,2,1,0:T(8,128)S(1)} fusion(bf16[2048,3072]{1,0:T(8,128)(2,1)} %all-gather.2.cloned.1.call-done, bf16[64,3072]{1,0:T(8,128)(2,1)S(1)} %subtract_convert_fusion, bf16[64,3072]{1,0:T(8,128)(2,1)} %param.13), kind=kOutput, calls=%fused_computation | convolution fusion | flops 1612185600 | bytes 14417920 | tf_op jit(solution)/shard_map/dot_general | solution.py:81
  112.0 1.1 copy.35
  113.1 6.5 %all-to-all-start = ((f32[16,128,128]{1,2,0:T(8,128)}), f32[16,128,128]{1,2,0:T(8,128)S(1)}, u32[]{:S(2)}, u32[]{:S(2)}) async-start(f32[16,128,128]{1,2,0:T(8,128)} %bitcast.10), calls=%async_computation | async-start | bytes 2097152 | tf_op jit(solution)/shard_map/all_to_all | solution.py:22
  119.6 16.4 %all-to-all-done = f32[16,128,128]{1,2,0:T(8,128)S(1)} async-done(((f32[16,128,128]{1,2,0:T(8,128)}), f32[16,128,128]{1,2,0:T(8,128)S(1)}, u32[]{:S(2)}, u32[]{:S(2)}) %all-to-all-start) | async-done | bytes 1048608 | tf_op jit(solution)/shard_map/all_to_all | solution.py:22
  136.4 11.1 %all_to_all.20 = f32[16,16,128]{2,1,0:T(8,128)S(1)} all-to-all(f32[16,16,128]{2,1,0:T(8,128)S(1)} %bitcast.13), channel_id=1, replica_groups=mesh['fs_0'=4,'fs_1'=4,'tp_0'=16,'tp_1'=2] {'fs_0','fs_1'}, dimensions={0} | all-to-all | bytes 262144 | tf_op jit(solution)/shard_map/all_to_all | solution.py:22
  147.7 9.9 %all_to_all.21 = f32[16,16,128]{2,1,0:T(8,128)S(1)} all-to-all(f32[16,16,128]{2,1,0:T(8,128)S(1)} %broadcast_in_dim.4), channel_id=1, replica_groups=mesh['fs_0'=4,'fs_1'=4,'tp_0'=16,'tp_1'=2] {'fs_0','fs_1'}, dimensions={0} | all-to-all | bytes 262144 | tf_op jit(solution)/shard_map/all_to_all | solution.py:28
  157.6 0.3 fusion.5
  157.9 0.6 multiply_reduce_fusion
  158.5 7.3 %all-reduce.2 = (f32[]{:T(128)}, f32[]{:T(128)}) all-reduce(f32[]{:T(128)} %get-tuple-element.25, f32[]{:T(128)} %get-tuple-element.24), channel_id=1, replica_groups=mesh['fs_0'=4,'fs_1'=4,'tp_0'=16,'tp_1'=2] {'fs_0'}, use_global_device_ids=true, to_apply=%region_4.5 | all-reduce | flops 2 | bytes 16 | tf_op jit(solution)/shard_map/psum | solution.py:46
  165.8 7.5 %all-reduce.1 = (f32[]{:T(128)}, f32[]{:T(128)}) all-reduce(f32[]{:T(128)} %get-tuple-element.30, f32[]{:T(128)} %get-tuple-element.31), channel_id=1, replica_groups=mesh['fs_0'=4,'fs_1'=4,'tp_0'=16,'tp_1'=2] {'fs_1'}, use_global_device_ids=true, to_apply=%region_5.6 | all-reduce | flops 2 | bytes 16 | tf_op jit(solution)/shard_map/psum | solution.py:46
  173.3 22.4 %all-reduce = (f32[]{:T(128)}, f32[]{:T(128)}) all-reduce(f32[]{:T(128)} %get-tuple-element.28, f32[]{:T(128)} %get-tuple-element.29), channel_id=1, replica_groups=mesh['fs_0'=4,'fs_1'=4,'tp_0'=16,'tp_1'=2] {'tp_0'}, use_global_device_ids=true, to_apply=%region_6.7 | all-reduce | flops 2 | bytes 16 | tf_op jit(solution)/shard_map/psum | solution.py:46
  195.6 16.8 %all-reduce.3 = (f32[]{:T(128)}, f32[]{:T(128)}) all-reduce(f32[]{:T(128)} %get-tuple-element.26, f32[]{:T(128)} %get-tuple-element.27), channel_id=1, replica_groups=mesh['fs_0'=4,'fs_1'=4,'tp_0'=16,'tp_1'=2] {'tp_1'}, use_global_device_ids=true, to_apply=%region_7.8 | all-reduce | flops 2 | bytes 16 | tf_op jit(solution)/shard_map/psum | solution.py:46
  213.8 0.6 fusion.16
  214.5 0.9 broadcast_in_dim.5
  215.4 3.6 %all-to-all-start.3 = ((bf16[16,128,128]{1,2,0:T(8,128)(2,1)}), bf16[16,128,128]{1,2,0:T(8,128)(2,1)S(1)}, u32[]{:S(2)}, u32[]{:S(2)}) async-start(bf16[16,128,128]{1,2,0:T(8,128)(2,1)} %broadcast_in_dim.5), calls=%async_computation.3 | async-start | bytes 1048576 | tf_op jit(solution)/shard_map/all_to_all | solution.py:28
  219.0 0.7 fusion.20
  219.6 10.3 %all-to-all-done.3 = bf16[16,128,128]{1,2,0:T(8,128)(2,1)S(1)} async-done(((bf16[16,128,128]{1,2,0:T(8,128)(2,1)}), bf16[16,128,128]{1,2,0:T(8,128)(2,1)S(1)}, u32[]{:S(2)}, u32[]{:S(2)}) %all-to-all-start.3) | async-done | bytes 524320 | tf_op jit(solution)/shard_map/all_to_all | solution.py:28
  229.9 0.3 copy.29
  230.4 0.9 copy.31
  231.3 0.9 copy.30
  (23 shorter events, 0.8 us)
Async XLA Ops:
  7.2 129.0 %copy-start = (bf16[2048,256]{1,0:T(8,128)(2,1)S(1)}, bf16[2048,256]{1,0:T(8,128)(2,1)}, u32[]{:S(2)}) copy-start(bf16[2048,256]{1,0:T(8,128)(2,1)} %param.17) | copy-start | bytes 3145732
  7.2 140.4 %copy-start.3 = (f32[16,64]{1,0:T(8,128)S(1)}, f32[16,64]{1,0:T(8,128)}, u32[]{:S(2)}) copy-start(f32[16,64]{1,0:T(8,128)} %param.23) | copy-start | bytes 12292
  7.2 140.4 %copy-start.5 = (f32[16,64]{1,0:T(8,128)S(1)}, f32[16,64]{1,0:T(8,128)}, u32[]{:S(2)}) copy-start(f32[16,64]{1,0:T(8,128)} %param.22) | copy-start | bytes 12292
  7.2 140.4 %copy-start.4 = (f32[16,64]{1,0:T(8,128)S(1)}, f32[16,64]{1,0:T(8,128)}, u32[]{:S(2)}) copy-start(f32[16,64]{1,0:T(8,128)} %param.21) | copy-start | bytes 12292
  7.2 140.4 %copy-start.6 = (f32[16,64]{1,0:T(8,128)S(1)}, f32[16,64]{1,0:T(8,128)}, u32[]{:S(2)}) copy-start(f32[16,64]{1,0:T(8,128)} %param.20) | copy-start | bytes 12292
  7.2 206.6 %copy-start.1 = (f32[128,64]{0,1:T(8,128)S(1)}, f32[128,64]{0,1:T(8,128)}, u32[]{:S(2)}) copy-start(f32[128,64]{0,1:T(8,128)} %param.19) | copy-start | bytes 98308
  7.2 206.6 %copy-start.2 = (f32[128,64]{0,1:T(8,128)S(1)}, f32[128,64]{0,1:T(8,128)}, u32[]{:S(2)}) copy-start(f32[128,64]{0,1:T(8,128)} %param.18) | copy-start | bytes 98308
  7.2 95.7 %all-gather.2.cloned.1.call-start = ((), (), s32[]{:S(2)}) async-start(), calls=%async_computation.4 | async-start | bytes 12976128 | tf_op jit(solution)/shard_map/all_gather | solution.py:82
  113.1 23.0 %all-to-all-start = ((f32[16,128,128]{1,2,0:T(8,128)}), f32[16,128,128]{1,2,0:T(8,128)S(1)}, u32[]{:S(2)}, u32[]{:S(2)}) async-start(f32[16,128,128]{1,2,0:T(8,128)} %bitcast.10), calls=%async_computation | async-start | bytes 2097152 | tf_op jit(solution)/shard_map/all_to_all | solution.py:22
  215.4 14.5 %all-to-all-start.3 = ((bf16[16,128,128]{1,2,0:T(8,128)(2,1)}), bf16[16,128,128]{1,2,0:T(8,128)(2,1)S(1)}, u32[]{:S(2)}, u32[]{:S(2)}) async-start(bf16[16,128,128]{1,2,0:T(8,128)(2,1)} %broadcast_in_dim.5), calls=%async_computation.3 | async-start | bytes 1048576 | tf_op jit(solution)/shard_map/all_to_all | solution.py:28
Sparse Core Ops, SparseCore 0:
  10.2 92.7 all-gather.1
where the time goes:
time: 240 us; the launch traced here: 239 us
  waiting for transfers between devices  120 us (50%)
  blocking collectives  74.9 us (31%)
  between operations  15.6 us (6%)
  starting transfers between devices  10.1 us (4%)
  matrix products  9.54 us (4%)
  local copies, waits for them, and re-layouts  5 us (2%)
  other arithmetic  3.48 us (1%)
    all_gather x1, waiting for transfers between devices, local(): lax.all_gather(normed, TP, axis=0, tiled=True)  92.9 us
    psum x4, blocking collectives, over_axes(): shard = lax.psum(shard, axis)  53.9 us
    all_to_all x1, waiting for transfers between devices, summed_on_arrival(): pieces = lax.all_to_all(cut_along(shard, dim, size), axis, 0, 0, tiled=True)  16.4 us
    all_to_all x1, blocking collectives, summed_on_arrival(): pieces = lax.all_to_all(cut_along(shard, dim, size), axis, 0, 0, tiled=True)  11.1 us
    all_to_all x1, waiting for transfers between devices, sent_to_all(): lax.all_to_all(jnp.broadcast_to(shard[None], (size, *shard.shape)), axis,...  10.3 us
    all_to_all x1, blocking collectives, sent_to_all(): lax.all_to_all(jnp.broadcast_to(shard[None], (size, *shard.shape)), axis,...  9.93 us
    dot_general x1, matrix products, local(): lax.dot_general(lax.all_gather(normed, TP, axis=0, tiled=True), cotangent...  8.99 us
    all_to_all x1, starting transfers between devices, summed_on_arrival(): pieces = lax.all_to_all(cut_along(shard, dim, size), axis, 0, 0, tiled=True)  6.53 us
  transfers between devices with their start and end apart: 3, of which 3 were waited for; matrix products, arithmetic and copies ran while one was open for 1% of the time, Pallas kernels for 0%

commit v1 on v0

--- a/solution.py
+++ b/solution.py
@@ -9,6 +9,13 @@
 TP = ("tp_0", "tp_1")
 FS = ("fs_0", "fs_1")
 FS_TP = ("fs_0", "fs_1", "tp_0", "tp_1")
+
+
+def swapped_in(x, axis, dim):
+    peers = lax.axis_size(axis)
+    pieces = jnp.stack([x for _ in range(peers)])
+    pieces = lax.all_to_all(pieces, axis, split_axis=0, concat_axis=0)
+    return jnp.concatenate(pieces, axis=dim)
 
 
 def cut_along(shard, dim, size):
@@ -79,7 +86,7 @@
         jnp.float32
     )
     term = lax.dot_general(
-        lax.all_gather(normed, TP, axis=0, tiled=True),
+        swapped_in(normed, TP, 0),
         cotangents,
         (((1,), (1,)), ((), ())),
         preferred_element_type=jnp.float32,

time: 240 us -> 703 us (2.93)
  waiting for transfers between devices: 120 us -> 564 us
  starting transfers between devices: 10.1 us -> 27.3 us
  between operations: 15.6 us -> 2.24 us
  blocking collectives: 74.9 us -> 85.7 us
  local copies, waits for them, and re-layouts: 5 us -> 12.2 us
    all_to_all x0 -> x1, waiting for transfers between devices: none -> 538 us  [swapped_in(): pieces = lax.all_to_all(pieces, axis, split_axis=0, concat_axis=0)]
    all_gather x1 -> x0, waiting for transfers between devices: 92.9 us -> none  [local(): lax.all_gather(normed, TP, axis=0, tiled=True)]
    all_to_all x0 -> x1, starting transfers between devices: none -> 16.9 us  [swapped_in(): pieces = lax.all_to_all(pieces, axis, split_axis=0, concat_axis=0)]
    psum x4, blocking collectives: 53.9 us -> 64.6 us  [over_axes(): shard = lax.psum(shard, axis)]
    another operation x0 -> x1, local copies, waits for them, and re-layouts: none -> 7.16 us  [swapped_in(): pieces = jnp.stack([x for _ in range(peers)])]
  transfers between devices with their start and end apart: 3 -> 3, of which waited for: 3 -> 3; matrix products, arithmetic and copies ran while one was open for 1% -> 0% of each run, Pallas kernels for 0% -> 0%
where the time goes in v1:
time: 703 us
  waiting for transfers between devices  564 us (80%)
  blocking collectives  85.7 us (12%)
  starting transfers between devices  27.3 us (4%)
  local copies, waits for them, and re-layouts  12.2 us (2%)
  matrix products  9.38 us (1%)
    all_to_all x1, waiting for transfers between devices, swapped_in(): pieces = lax.all_to_all(pieces, axis, split_axis=0, concat_axis=0)  538 us
    psum x4, blocking collectives, over_axes(): shard = lax.psum(shard, axis)  64.6 us
    all_to_all x1, starting transfers between devices, swapped_in(): pieces = lax.all_to_all(pieces, axis, split_axis=0, concat_axis=0)  16.9 us
    all_to_all x1, waiting for transfers between devices, summed_on_arrival(): pieces = lax.all_to_all(cut_along(shard, dim, size), axis, 0, 0, tiled=True)  16.2 us
  transfers between devices with their start and end apart: 3, of which 3 were waited for; matrix products, arithmetic and copies ran while one was open for 0% of the time, Pallas kernels for 0%

profile of v1, /device:TPU:1, one launch (start us, length us, event | category | flops | bytes accessed | tf_op | source)
XLA Modules:
  0.0 702.8 jit_solution(15912685589081085342)
XLA Ops:
  0.6 7.2 %stack.2 = bf16[32,64,3072]{2,1,0:T(8,128)(2,1)} broadcast(bf16[64,3072]{1,0:T(8,128)(2,1)} %param.12), dimensions={1,2} | broadcast | bytes 12976128 | tf_op jit(solution)/shard_map/stack | solution.py:16
  7.8 16.9 %all-to-all-start = ((bf16[32,64,3072]{2,1,0:T(8,128)(2,1)}), bf16[32,64,3072]{2,1,0:T(8,128)(2,1)}, u32[]{:S(2)}, u32[]{:S(2)}) async-start(bf16[32,64,3072]{2,1,0:T(8,128)(2,1)} %stack.2), calls=%async_computation | async-start | bytes 25165824 | tf_op jit(solution)/shard_map/all_to_all | solution.py:17
  25.1 537.9 %all-to-all-done = bf16[32,64,3072]{2,1,0:T(8,128)(2,1)} async-done(((bf16[32,64,3072]{2,1,0:T(8,128)(2,1)}), bf16[32,64,3072]{2,1,0:T(8,128)(2,1)}, u32[]{:S(2)}, u32[]{:S(2)}) %all-to-all-start) | async-done | bytes 12582944 | tf_op jit(solution)/shard_map/all_to_all | solution.py:17
  563.0 8.8 %convolution_bitcast_fusion = f32[16,16,8,128]{3,2,1,0:T(8,128)S(1)} fusion(bf16[2048,3072]{1,0:T(8,128)(2,1)} %bitcast, bf16[64,3072]{1,0:T(8,128)(2,1)S(1)} %subtract_convert_fusion, bf16[64,3072]{1,0:T(8,128)(2,1)S(1)} %copy-done.1), kind=kOutput, calls=%fused_computation | convolution fusion | flops 1612185600 | bytes 14417920 | tf_op jit(solution)/shard_map/dot_general | solution.py:88
  571.9 1.1 copy.35
  573.0 6.8 all-to-all-start.1
  579.7 16.2 %all-to-all-done.1 = f32[16,128,128]{1,2,0:T(8,128)S(1)} async-done(((f32[16,128,128]{1,2,0:T(8,128)}), f32[16,128,128]{1,2,0:T(8,128)S(1)}, u32[]{:S(2)}, u32[]{:S(2)}) %all-to-all-start.1) | async-done | bytes 1048608 | tf_op jit(solution)/shard_map/all_to_all | solution.py:29
  596.0 0.3 fusion.3
  596.3 11.2 %all_to_all.25 = f32[16,16,128]{2,1,0:T(8,128)S(1)} all-to-all(f32[16,16,128]{2,1,0:T(8,128)S(1)} %bitcast.14), channel_id=1, replica_groups=mesh['fs_0'=4,'fs_1'=4,'tp_0'=16,'tp_1'=2] {'fs_0','fs_1'}, dimensions={0} | all-to-all | bytes 262144 | tf_op jit(solution)/shard_map/all_to_all | solution.py:29
  607.6 9.9 %all_to_all.26 = f32[16,16,128]{2,1,0:T(8,128)S(1)} all-to-all(f32[16,16,128]{2,1,0:T(8,128)S(1)} %broadcast_in_dim.4), channel_id=1, replica_groups=mesh['fs_0'=4,'fs_1'=4,'tp_0'=16,'tp_1'=2] {'fs_0','fs_1'}, dimensions={0} | all-to-all | bytes 262144 | tf_op jit(solution)/shard_map/all_to_all | solution.py:35
  617.6 0.3 fusion.5
  617.9 0.6 multiply_reduce_fusion
  618.5 7.3 %all-reduce.2 = (f32[]{:T(128)}, f32[]{:T(128)}) all-reduce(f32[]{:T(128)} %get-tuple-element.25, f32[]{:T(128)} %get-tuple-element.24), channel_id=1, replica_groups=mesh['fs_0'=4,'fs_1'=4,'tp_0'=16,'tp_1'=2] {'fs_0'}, use_global_device_ids=true, to_apply=%region_4.5 | all-reduce | flops 2 | bytes 16 | tf_op jit(solution)/shard_map/psum | solution.py:53
  625.7 7.5 %all-reduce.1 = (f32[]{:T(128)}, f32[]{:T(128)}) all-reduce(f32[]{:T(128)} %get-tuple-element.30, f32[]{:T(128)} %get-tuple-element.31), channel_id=1, replica_groups=mesh['fs_0'=4,'fs_1'=4,'tp_0'=16,'tp_1'=2] {'fs_1'}, use_global_device_ids=true, to_apply=%region_5.6 | all-reduce | flops 2 | bytes 16 | tf_op jit(solution)/shard_map/psum | solution.py:53
  633.2 32.1 %all-reduce = (f32[]{:T(128)}, f32[]{:T(128)}) all-reduce(f32[]{:T(128)} %get-tuple-element.28, f32[]{:T(128)} %get-tuple-element.29), channel_id=1, replica_groups=mesh['fs_0'=4,'fs_1'=4,'tp_0'=16,'tp_1'=2] {'tp_0'}, use_global_device_ids=true, to_apply=%region_6.7 | all-reduce | flops 2 | bytes 16 | tf_op jit(solution)/shard_map/psum | solution.py:53
  665.3 17.7 %all-reduce.3 = (f32[]{:T(128)}, f32[]{:T(128)}) all-reduce(f32[]{:T(128)} %get-tuple-element.26, f32[]{:T(128)} %get-tuple-element.27), channel_id=1, replica_groups=mesh['fs_0'=4,'fs_1'=4,'tp_0'=16,'tp_1'=2] {'tp_1'}, use_global_device_ids=true, to_apply=%region_7.8 | all-reduce | flops 2 | bytes 16 | tf_op jit(solution)/shard_map/psum | solution.py:53
  684.4 0.6 fusion.16
  685.1 0.9 broadcast_in_dim.5
  686.0 3.6 all-to-all-start.4
  689.5 0.7 fusion.20
  690.2 10.3 %all-to-all-done.4 = bf16[16,128,128]{1,2,0:T(8,128)(2,1)S(1)} async-done(((bf16[16,128,128]{1,2,0:T(8,128)(2,1)}), bf16[16,128,128]{1,2,0:T(8,128)(2,1)S(1)}, u32[]{:S(2)}, u32[]{:S(2)}) %all-to-all-start.4) | async-done | bytes 524320 | tf_op jit(solution)/shard_map/all_to_all | solution.py:35
  700.5 0.3 copy.29
  701.0 0.9 copy.30
  701.9 0.9 copy.31
  (31 shorter events, 0.7 us)
Async XLA Ops:
  0.6 595.4 %copy-start = (bf16[2048,256]{1,0:T(8,128)(2,1)S(1)}, bf16[2048,256]{1,0:T(8,128)(2,1)}, u32[]{:S(2)}) copy-start(bf16[2048,256]{1,0:T(8,128)(2,1)} %param.17) | copy-start | bytes 3145732
  7.8 17.0 %copy-start.10 = (f32[8]{0:T(128)S(1)}, f32[8]{0:T(128)}, u32[]{:S(2)}) copy-start(f32[8]{0:T(128)} %param.16) | copy-start | bytes 100
  7.8 17.1 %copy-start.2 = (bf16[64,3072]{1,0:T(8,128)(2,1)S(1)}, bf16[64,3072]{1,0:T(8,128)(2,1)}, u32[]{:S(2)}) copy-start(bf16[64,3072]{1,0:T(8,128)(2,1)} %param.15) | copy-start | bytes 1179652
  7.8 17.1 %copy-start.3 = (bf16[64,3072]{1,0:T(8,128)(2,1)S(1)}, bf16[64,3072]{1,0:T(8,128)(2,1)}, u32[]{:S(2)}) copy-start(bf16[64,3072]{1,0:T(8,128)(2,1)} %param.14) | copy-start | bytes 1179652
  7.8 555.2 %copy-start.1 = (bf16[64,3072]{1,0:T(8,128)(2,1)S(1)}, bf16[64,3072]{1,0:T(8,128)(2,1)}, u32[]{:S(2)}) copy-start(bf16[64,3072]{1,0:T(8,128)(2,1)} %param.13) | copy-start | bytes 1179652
  7.8 555.2 %all-to-all-start = ((bf16[32,64,3072]{2,1,0:T(8,128)(2,1)}), bf16[32,64,3072]{2,1,0:T(8,128)(2,1)}, u32[]{:S(2)}, u32[]{:S(2)}) async-start(bf16[32,64,3072]{2,1,0:T(8,128)(2,1)} %stack.2), calls=%async_computation | async-start | bytes 25165824 | tf_op jit(solution)/shard_map/all_to_all | solution.py:17
  24.8 582.7 %copy-start.6 = (f32[16,64]{1,0:T(8,128)S(1)}, f32[16,64]{1,0:T(8,128)}, u32[]{:S(2)}) copy-start(f32[16,64]{1,0:T(8,128)} %param.23) | copy-start | bytes 12292
  24.8 582.7 %copy-start.7 = (f32[16,64]{1,0:T(8,128)S(1)}, f32[16,64]{1,0:T(8,128)}, u32[]{:S(2)}) copy-start(f32[16,64]{1,0:T(8,128)} %param.21) | copy-start | bytes 12292
  24.8 582.7 %copy-start.8 = (f32[16,64]{1,0:T(8,128)S(1)}, f32[16,64]{1,0:T(8,128)}, u32[]{:S(2)}) copy-start(f32[16,64]{1,0:T(8,128)} %param.22) | copy-start | bytes 12292
  24.8 582.7 %copy-start.9 = (f32[16,64]{1,0:T(8,128)S(1)}, f32[16,64]{1,0:T(8,128)}, u32[]{:S(2)}) copy-start(f32[16,64]{1,0:T(8,128)} %param.20) | copy-start | bytes 12292
  24.8 659.6 %copy-start.4 = (f32[128,64]{0,1:T(8,128)S(1)}, f32[128,64]{0,1:T(8,128)}, u32[]{:S(2)}) copy-start(f32[128,64]{0,1:T(8,128)} %param.19) | copy-start | bytes 98308
  24.8 659.6 %copy-start.5 = (f32[128,64]{0,1:T(8,128)S(1)}, f32[128,64]{0,1:T(8,128)}, u32[]{:S(2)}) copy-start(f32[128,64]{0,1:T(8,128)} %param.18) | copy-start | bytes 98308
  573.0 23.0 %all-to-all-start.1 = ((f32[16,128,128]{1,2,0:T(8,128)}), f32[16,128,128]{1,2,0:T(8,128)S(1)}, u32[]{:S(2)}, u32[]{:S(2)}) async-start(f32[16,128,128]{1,2,0:T(8,128)} %bitcast.11), calls=%async_computation.1 | async-start | bytes 2097152 | tf_op jit(solution)/shard_map/all_to_all | solution.py:29
  686.0 14.5 %all-to-all-start.4 = ((bf16[16,128,128]{1,2,0:T(8,128)(2,1)}), bf16[16,128,128]{1,2,0:T(8,128)(2,1)S(1)}, u32[]{:S(2)}, u32[]{:S(2)}) async-start(bf16[16,128,128]{1,2,0:T(8,128)(2,1)} %broadcast_in_dim.5), calls=%async_computation.4 | async-start | bytes 1048576 | tf_op jit(solution)/shard_map/all_to_all | solution.py:35
